TPU v7x, 32 devices: a whole 2x2x4 slice. The times are simulated.
32 devices in a mesh: sp: 8 (over z, x), tp: 4 (over y, core).
Axes of the slice: x: 2, y: 2, z: 4, core: 2. Of those that a mesh axis runs over, the one named last changes fastest.
Arguments:
- moe_in: bfloat16 [1536, 2048], P('sp', 'tp'), may hold values from -6 to 6
- cotangent: bfloat16 [1536, 2048], P('sp', 'tp'), may hold values from -6 to 6
- routes: int32 [1536, 2], P('sp'), may hold values from 0 to 7, all different within a row; in each aligned block of 192 rows (0 to 191, 192 to 383, ...) at most 60 rows name the same one
- route_weight: float32 [1536, 2], P('sp'), may hold values from 0.2 to 1
- w_gate: bfloat16 [8, 3584, 2048], P('sp', 'tp'), may hold values from -0.125 to 0.125
- w_up: bfloat16 [8, 3584, 2048], P('sp', 'tp'), may hold values from -0.125 to 0.125
- w_down: bfloat16 [8, 3584, 2048], P('sp', 'tp'), may hold values from -0.09375 to 0.09375
- conv_pre: bfloat16 [1536, 2048], P('sp', 'tp'), may hold values from -6 to 6
- norm_mean: float32 [1536], P('sp'), may hold values from -3 to 3
- norm_rstd: float32 [1536], P('sp'), may hold values from 0.5 to 2
- ln_gain: float32 [2048], P('tp'), may hold values from 0.1 to 1.9
- ln_shift: float32 [2048], P('tp'), may hold values from -3 to 3
- taps: float32 [31, 2048], P(None, 'tp'), may hold values from -1 to 1
- w_proj: bfloat16 [2048, 2048], P('sp', 'tp'), may hold values from -0.125 to 0.125
Outputs:
- grad_up: bfloat16 [8, 3584, 2048], P('sp', 'tp')
- grad_down: bfloat16 [8, 3584, 2048], P('sp', 'tp')
- grad_stream: bfloat16 [1536, 2048], P('sp', 'tp')
- grad_proj: float32 [2048, 2048], P('sp', 'tp')
- grad_conv: bfloat16 [1536, 2048], P('sp', 'tp')
Inputs may be any that keep to these rules, and one draw needn't show every extreme that they name: `routes`: each token names 2 different experts. Among the tokens of one index of sp no expert is named more than 60 times, a bound that some block reaches.
All inputs are finite; a program needn't handle non-finite values.
Results may differ from a plain program's by a relative error of at most 0.02.
Values may be sent and summed in bfloat16 or wider, within the bound.
A program may use at most 64 MiB of HBM per device.

v0:
```python
import jax
import jax.numpy as jnp
from jax import lax
from jax.sharding import PartitionSpec as P


def passed_along(value, axis, steps):
    count = lax.axis_size(axis)
    first, last = (max(0, -steps), min(count, count - steps))
    return lax.ppermute(value, axis, [(source, source + steps) for source in range(first, last)])


def silu_slope(pre_value, sigmoid_value):
    return sigmoid_value * (1.0 + pre_value * (1.0 - sigmoid_value))


def expert_backward(expert_rows, routed_rows, gate_weight, up_weight, down_weight):
    gate_pre = lax.dot_general(
        expert_rows, gate_weight, (((1,), (1,)), ((), ())), preferred_element_type=jnp.float32
    )
    up_pre = lax.dot_general(
        expert_rows, up_weight, (((1,), (1,)), ((), ())), preferred_element_type=jnp.float32
    )
    gate_sigmoid = jax.nn.sigmoid(gate_pre)
    gate_active = gate_pre * gate_sigmoid
    hidden = (gate_active * up_pre).astype(jnp.bfloat16)
    hidden_grad = lax.dot_general(
        routed_rows, down_weight, (((1,), (1,)), ((), ())), preferred_element_type=jnp.float32
    )
    grad_down = lax.dot_general(
        hidden, routed_rows, (((0,), (0,)), ((), ())), preferred_element_type=jnp.float32
    ).astype(jnp.bfloat16)
    gate_grad = (hidden_grad * up_pre * silu_slope(gate_pre, gate_sigmoid)).astype(jnp.bfloat16)
    up_grad = (hidden_grad * gate_active).astype(jnp.bfloat16)
    grad_up = lax.dot_general(
        up_grad, expert_rows, (((0,), (0,)), ((), ())), preferred_element_type=jnp.float32
    ).astype(jnp.bfloat16)
    partial_rows = jnp.dot(gate_grad, gate_weight, preferred_element_type=jnp.float32)
    partial_rows = partial_rows + jnp.dot(up_grad, up_weight, preferred_element_type=jnp.float32)
    return (grad_up[None], grad_down[None], partial_rows)


def on_device(
    moe_in,
    cotangent,
    routes,
    route_weight,
    w_gate,
    w_up,
    w_down,
    conv_pre,
    norm_mean,
    norm_rstd,
    ln_gain,
    ln_shift,
    taps,
    w_proj,
):
    devices = lax.axis_size("sp")
    local_tokens = routes.shape[0]
    top_count = routes.shape[1]
    channels = moe_in.shape[1]
    capacity = 5 * local_tokens // (2 * devices)
    route_ids = routes.reshape(-1)
    onehot = (route_ids[:, None] == jnp.arange(devices, dtype=jnp.int32)[None, :]).astype(jnp.int32)
    earlier = jnp.cumsum(onehot, axis=0) - onehot
    targets = route_ids * capacity + jnp.sum(earlier * onehot, axis=1)
    positions = jnp.arange(devices * capacity, dtype=jnp.int32)
    matches = targets[None, :] == positions[:, None]
    filled = jnp.any(matches, axis=1)[:, None]
    pair_index = jnp.arange(targets.shape[0], dtype=jnp.int32)
    route_of_slot = jnp.sum(jnp.where(matches, pair_index[None, :], 0), axis=1)
    zero_value = jnp.zeros((), jnp.bfloat16)
    routed = (route_weight[:, :, None] * cotangent.astype(jnp.float32)[:, None, :]).astype(
        jnp.bfloat16
    )
    routed = routed.reshape(local_tokens * top_count, cotangent.shape[1])
    send_rows = jnp.where(filled, jnp.take(moe_in, route_of_slot // top_count, axis=0), zero_value)
    send_routed = jnp.where(filled, jnp.take(routed, route_of_slot, axis=0), zero_value)
    send_rows, send_routed = (send_rows, send_routed)
    part_rows, part_routed = (
        lax.all_to_all(send_rows, "sp", split_axis=0, concat_axis=0, tiled=True),
        lax.all_to_all(send_routed, "sp", split_axis=0, concat_axis=0, tiled=True),
    )
    expert_rows, routed_rows = (
        lax.all_gather(part_rows, "tp", axis=1, tiled=True),
        lax.all_gather(part_routed, "tp", axis=1, tiled=True),
    )
    grad_up, grad_down, partial_rows = expert_backward(
        expert_rows, routed_rows, w_gate[0], w_up[0], w_down[0]
    )
    shared = lax.psum_scatter(
        partial_rows.astype(jnp.bfloat16).astype(jnp.float32).astype(jnp.bfloat16),
        "tp",
        scatter_dimension=1,
        tiled=True,
    )
    returned = lax.all_to_all(shared, "sp", split_axis=0, concat_axis=0, tiled=True)
    picked = jnp.take(returned, targets, axis=0).astype(jnp.float32)
    grad_stream = (
        cotangent.astype(jnp.float32)
        + jnp.sum(picked.reshape(local_tokens, top_count, returned.shape[1]), axis=1)
    ).astype(jnp.bfloat16)
    mix_grad = lax.all_gather(grad_stream, "tp", axis=1, tiled=True)
    normed = (conv_pre.astype(jnp.float32) - norm_mean[:, None]) * norm_rstd[:, None]
    pre_act = normed * ln_gain[None, :] + ln_shift[None, :]
    act_sigmoid = jax.nn.sigmoid(pre_act)
    activated = (pre_act * act_sigmoid).astype(jnp.bfloat16)
    columns = mix_grad
    act_grad = jnp.dot(
        columns,
        lax.all_gather(w_proj, "sp", axis=0, tiled=True),
        preferred_element_type=jnp.float32,
    )
    columns = mix_grad
    grad_proj = lax.psum_scatter(
        lax.dot_general(
            columns, activated, (((0,), (0,)), ((), ())), preferred_element_type=jnp.float32
        ).astype(jnp.bfloat16),
        "sp",
        scatter_dimension=0,
        tiled=True,
    ).astype(jnp.float32)
    normed_grad = act_grad * silu_slope(pre_act, act_sigmoid) * ln_gain[None, :]
    first_sum, second_sum = lax.psum(
        (jnp.sum(normed_grad, axis=1), jnp.sum(normed_grad * normed, axis=1)), "tp"
    )
    width = channels * lax.axis_size("tp")
    conv_grad = norm_rstd[:, None] * (
        normed_grad - first_sum[:, None] / width - normed * (second_sum[:, None] / width)
    )
    lag_count = taps.shape[0]
    rim_rows = passed_along(conv_grad[: lag_count - 1], "sp", -1)
    extended = jnp.concatenate([conv_grad, rim_rows], axis=0)
    grad_conv = jnp.zeros((local_tokens, channels), jnp.float32)
    for lag in range(lag_count):
        grad_conv = grad_conv + taps[lag][None, :] * extended[lag : lag + local_tokens]
    return (grad_up, grad_down, grad_stream, grad_proj, grad_conv.astype(jnp.bfloat16))


def solution(mesh):
    placed = (
        P("sp", "tp"),
        P("sp", "tp"),
        P("sp", None),
        P("sp", None),
        P("sp", "tp", None),
        P("sp", "tp", None),
        P("sp", "tp", None),
        P("sp", "tp"),
        P("sp"),
        P("sp"),
        P("tp"),
        P("tp"),
        P(None, "tp"),
        P("sp", "tp"),
    )
    return jax.shard_map(
        on_device,
        mesh=mesh,
        in_specs=placed,
        out_specs=(
            P("sp", "tp", None),
            P("sp", "tp", None),
            P("sp", "tp"),
            P("sp", "tp"),
            P("sp", "tp"),
        ),
        check_vma=False,
    )
```

profile of v0, /device:TPU:0, one launch (start us, length us, event | category | flops | bytes accessed | tf_op | source)
XLA Modules:
  0.0 252.3 jit_solution(15839050493758933226)
XLA Ops:
  12.9 2.1 gather_fusion
  15.2 2.1 gather_fusion.1
  17.8 21.6 %all_to_all.30 = bf16[8,60,512]{2,1,0:T(8,128)(2,1)S(1)} all-to-all(bf16[8,60,512]{2,1,0:T(8,128)(2,1)S(1)} %get-tuple-element.44), channel_id=1, replica_groups=mesh['sp'=8,'tp'=4] {'sp'}, dimensions={0} | all-to-all | bytes 983040 | tf_op jit(solution)/shard_map/all_to_all | solution.py:82
  40.4 17.5 %all_to_all.31 = bf16[8,60,512]{2,1,0:T(8,128)(2,1)S(1)} all-to-all(bf16[8,60,512]{2,1,0:T(8,128)(2,1)S(1)} %get-tuple-element.45), channel_id=1, replica_groups=mesh['sp'=8,'tp'=4] {'sp'}, dimensions={0} | all-to-all | bytes 983040 | tf_op jit(solution)/shard_map/all_to_all | solution.py:83
  59.0 2.3 all-gather.6.cloned.1.call-done
  61.4 4.9 %fusion.6 = f32[480,896]{1,0:T(8,128)S(1)} fusion(bf16[480,2048]{1,0:T(8,128)(2,1)} %all-gather.6.cloned.1.call-done, bf16[1,896,2048]{2,1,0:T(8,128)(2,1)} %param.18), kind=kOutput, calls=%fused_computation.39 | convolution fusion | flops 1761607680 | bytes 7356416 | tf_op jit(solution)/shard_map/dot_general | solution.py:18
  66.2 19.1 %all-gather.4.cloned.1.call-done = bf16[480,2048]{1,0:T(8,128)(2,1)} async-done(((bf16[480,512]{1,0:T(8,128)(2,1)}), bf16[480,2048]{1,0:T(8,128)(2,1)}) %all-gather.4.cloned.1.call-update) | async-done | bytes 1966096 | tf_op jit(solution)/shard_map/all_gather | solution.py:87
  85.4 5.1 %multiply_convert_fusion.2 = (bf16[480,896]{1,0:T(8,128)(2,1)S(1)}, f32[480,896]{1,0:T(8,128)S(1)}) fusion(f32[480,896]{1,0:T(8,128)S(1)} %fusion.6, bf16[480,2048]{1,0:T(8,128)(2,1)} %all-gather.4.cloned.1.call-done, bf16[1,896,2048]{2,1,0:T(8,128)(2,1)} %param.20), kind=kOutput, calls=%fused_computation.48 | convolution fusion | flops 1764188160 | bytes 9936896 | tf_op jit(solution)/shard_map/dot_general | solution.py:27
  91.4 2.2 fusion
  93.6 2.3 fusion.2
  97.1 3.7 %add_convert_fusion = bf16[480,2048]{1,0:T(8,128)(2,1)} fusion(f32[480,2048]{1,0:T(8,128)S(1)} %fusion, bf16[1,896,2048]{2,1,0:T(8,128)(2,1)S(1)} %copy-done.10, f32[480,896]{1,0:T(8,128)S(1)} %fusion.6, f32[480,896]{1,0:T(8,128)S(1)} %get-tuple-element.47, f32[480,896]{1,0:T(8,128)S(1)} %fusion.2), kind=kOutput, calls=%fused_computation.32 | convolution fusion | flops 1767874560 | bytes 14729216 | tf_op jit(solution)/shard_map/dot_general | solution.py:38
  101.4 30.0 %reduce-scatter.3.cloned.1.call-done = bf16[480,512]{1,0:T(8,128)(2,1)} async-done(((bf16[480,2048]{1,0:T(8,128)(2,1)}), bf16[480,512]{1,0:T(8,128)(2,1)}) %reduce-scatter.3.cloned.1.call-update) | async-done | bytes 491536 | tf_op jit(solution)/shard_map/reduce_scatter | solution.py:92
  131.4 1.9 all_to_all.24
  133.3 5.5 %all-to-all-start.2 = ((bf16[8,60,512]{2,1,0:T(8,128)(2,1)}), bf16[8,60,512]{2,1,0:T(8,128)(2,1)S(1)}, u32[]{:S(2)}, u32[]{:S(2)}) async-start(bf16[8,60,512]{2,1,0:T(8,128)(2,1)} %all_to_all.24), calls=%async_computation.3 | async-start | bytes 1048576 | tf_op jit(solution)/shard_map/all_to_all | solution.py:98
  139.6 21.8 %all-to-all-done.2 = bf16[8,60,512]{2,1,0:T(8,128)(2,1)S(1)} async-done(((bf16[8,60,512]{2,1,0:T(8,128)(2,1)}), bf16[8,60,512]{2,1,0:T(8,128)(2,1)S(1)}, u32[]{:S(2)}, u32[]{:S(2)}) %all-to-all-start.2) | async-done | bytes 491552 | tf_op jit(solution)/shard_map/all_to_all | solution.py:98
  161.5 2.1 gather_fusion.2
  165.0 8.4 %all_gather.14 = bf16[192,2048]{1,0:T(8,128)(2,1)S(1)} all-gather(bf16[192,512]{1,0:T(8,128)(2,1)S(1)} %add_convert_fusion.1), channel_id=1, replica_groups=mesh['sp'=8,'tp'=4] {'tp'}, dimensions={1}, use_global_device_ids=true | all-gather | bytes 983040 | tf_op jit(solution)/shard_map/all_gather | solution.py:104
  173.4 2.3 convolution_convert_fusion
  177.3 6.0 %convert_bitcast_fusion = bf16[1,896,2048]{2,1,0:T(8,128)(2,1)} fusion(bf16[480,2048]{1,0:T(8,128)(2,1)S(1)} %copy-done.12, f32[480,896]{1,0:T(8,128)} %copy-done.16, f32[480,896]{1,0:T(8,128)} %copy-done.15), kind=kOutput, calls=%fused_computation.43 | convolution fusion | flops 1766023168 | bytes 9076736 | tf_op jit(solution)/shard_map/dot_general | solution.py:30
  183.3 2.5 fusion.121
  185.8 7.0 %all-reduce = (f32[192]{0:T(256)S(1)}, f32[192]{0:T(256)S(1)}) all-reduce(f32[192]{0:T(256)S(1)} %get-tuple-element.6, f32[192]{0:T(256)S(1)} %get-tuple-element.5), channel_id=1, replica_groups=mesh['sp'=8,'tp'=4] {'tp'}, use_global_device_ids=true, to_apply=%region_11.12 | all-reduce | flops 384 | bytes 3072 | tf_op jit(solution)/shard_map/psum | solution.py:125
  194.2 5.5 %convert_bitcast_fusion.1 = bf16[1,896,2048]{2,1,0:T(8,128)(2,1)} fusion(bf16[480,896]{1,0:T(8,128)(2,1)S(1)} %copy-done.18, bf16[480,2048]{1,0:T(8,128)(2,1)} %all-gather.6.cloned.1.call-done), kind=kOutput, calls=%fused_computation.44 | convolution fusion | flops 1763442688 | bytes 6496256 | tf_op jit(solution)/shard_map/dot_general | solution.py:35
  199.8 2.5 fusion.20
  202.3 41.1 %reduce-scatter.5.cloned.1.call-done = bf16[256,512]{1,0:T(8,128)(2,1)} async-done(((bf16[2048,512]{1,0:T(8,128)(2,1)}), bf16[256,512]{1,0:T(8,128)(2,1)}) %reduce-scatter.5.cloned.1.call-update) | async-done | bytes 262160 | tf_op jit(solution)/shard_map/reduce_scatter | solution.py:116
  (97 shorter events, 17.2 us)
Async XLA Ops:
  8.0 7.2 %copy-start = (bf16[192,512]{1,0:T(8,128)(2,1)S(1)}, bf16[192,512]{1,0:T(8,128)(2,1)}, u32[]{:S(2)}) copy-start(bf16[192,512]{1,0:T(8,128)(2,1)} %param.14) | copy-start | bytes 589828
  8.0 4.5 %copy-start.6 = (f32[192,2]{0,1:T(2,128)S(1)}, f32[192,2]{0,1:T(2,128)}, u32[]{:S(2)}) copy-start(f32[192,2]{0,1:T(2,128)} %param.17) | copy-start | bytes 4612
  8.0 53.3 %all-gather.6.cloned.1.call-start = ((), (), s32[]{:S(2)}) async-start(), calls=%async_computation.6 | async-start | bytes 2457600 | tf_op jit(solution)/shard_map/all_gather | solution.py:86
  40.3 45.0 %all-gather.4.cloned.1.call-start = ((), (), s32[]{:S(2)}) async-start(), calls=%async_computation.5 | async-start | bytes 2457600 | tf_op jit(solution)/shard_map/all_gather | solution.py:87
  58.8 72.6 %reduce-scatter.3.cloned.1.call-start = ((), (), s32[]{:S(2)}) async-start(), calls=%async_computation.7 | async-start | bytes 2457600 | tf_op jit(solution)/shard_map/reduce_scatter | solution.py:92
  66.2 29.7 %copy-start.15 = (f32[480,896]{1,0:T(8,128)}, f32[480,896]{1,0:T(8,128)S(1)}, u32[]{:S(2)}) copy-start(f32[480,896]{1,0:T(8,128)S(1)} %fusion.6) | copy-start | bytes 5160964
  85.3 6.0 %copy-start.9 = (bf16[1,896,2048]{2,1,0:T(8,128)(2,1)S(1)}, bf16[1,896,2048]{2,1,0:T(8,128)(2,1)}, u32[]{:S(2)}) copy-start(bf16[1,896,2048]{2,1,0:T(8,128)(2,1)} %param.19) | copy-start | bytes 11010052
  91.4 2.2 copy-start.11
  93.6 3.5 %copy-start.10 = (bf16[1,896,2048]{2,1,0:T(8,128)(2,1)S(1)}, bf16[1,896,2048]{2,1,0:T(8,128)(2,1)}, u32[]{:S(2)}) copy-start(bf16[1,896,2048]{2,1,0:T(8,128)(2,1)} %param.18) | copy-start | bytes 11010052
  95.9 1.2 copy-start.16
  100.8 38.2 %copy-start.5 = (s32[192,2]{0,1:T(2,128)S(1)}, s32[192,2]{0,1:T(2,128)}, u32[]{:S(2)}) copy-start(s32[192,2]{0,1:T(2,128)} %param.16) | copy-start | bytes 4612
  100.9 82.4 %all-gather.8.cloned.1.call-start = ((), (), s32[]{:S(2)}) async-start(), calls=%async_computation.9 | async-start | bytes 2359296 | tf_op jit(solution)/shard_map/all_gather | solution.py:112
  133.3 28.1 %all-to-all-start.2 = ((bf16[8,60,512]{2,1,0:T(8,128)(2,1)}), bf16[8,60,512]{2,1,0:T(8,128)(2,1)S(1)}, u32[]{:S(2)}, u32[]{:S(2)}) async-start(bf16[8,60,512]{2,1,0:T(8,128)(2,1)} %all_to_all.24), calls=%async_computation.3 | async-start | bytes 1048576 | tf_op jit(solution)/shard_map/all_to_all | solution.py:98
  138.8 104.6 %reduce-scatter.5.cloned.1.call-start = ((), (), s32[]{:S(2)}) async-start(), calls=%async_computation.8 | async-start | bytes 2359296 | tf_op jit(solution)/shard_map/reduce_scatter | solution.py:116
  161.5 3.4 %copy-start.1 = (bf16[192,512]{1,0:T(8,128)(2,1)S(1)}, bf16[192,512]{1,0:T(8,128)(2,1)}, u32[]{:S(2)}) copy-start(bf16[192,512]{1,0:T(8,128)(2,1)} %param.15) | copy-start | bytes 589828
  163.6 9.8 %copy-start.3 = (bf16[192,512]{1,0:T(8,128)(2,1)S(1)}, bf16[192,512]{1,0:T(8,128)(2,1)}, u32[]{:S(2)}) copy-start(bf16[192,512]{1,0:T(8,128)(2,1)} %param.21) | copy-start | bytes 589828
  163.6 9.8 %copy-start.7 = (f32[192]{0:T(256)S(1)}, f32[192]{0:T(256)}, u32[]{:S(2)}) copy-start(f32[192]{0:T(256)} %param.23) | copy-start | bytes 2308
  163.6 9.8 %copy-start.8 = (f32[192]{0:T(256)S(1)}, f32[192]{0:T(256)}, u32[]{:S(2)}) copy-start(f32[192]{0:T(256)} %param.22) | copy-start | bytes 2308
  163.6 9.8 %copy-start.13 = (f32[512]{0:T(512)S(1)}, f32[512]{0:T(512)}, u32[]{:S(2)}) copy-start(f32[512]{0:T(512)} %param.25) | copy-start | bytes 6148
  163.6 9.8 %copy-start.14 = (f32[512]{0:T(512)S(1)}, f32[512]{0:T(512)}, u32[]{:S(2)}) copy-start(f32[512]{0:T(512)} %param.24) | copy-start | bytes 6148
  165.0 10.7 %copy-start.2 = (bf16[192,512]{1,0:T(8,128)(2,1)}, bf16[192,512]{1,0:T(8,128)(2,1)S(1)}, u32[]{:S(2)}) copy-start(bf16[192,512]{1,0:T(8,128)(2,1)S(1)} %add_convert_fusion.1) | copy-start | bytes 589828
  175.7 1.6 copy-start.12
  183.3 10.9 %copy-start.18 = (bf16[480,896]{1,0:T(8,128)(2,1)S(1)}, bf16[480,896]{1,0:T(8,128)(2,1)}, u32[]{:S(2)}) copy-start(bf16[480,896]{1,0:T(8,128)(2,1)} %copy-done.17) | copy-start | bytes 2580484
  192.9 6.9 %collective-permute-start = (f32[30,512]{1,0:T(8,128)S(1)}, f32[30,512]{1,0:T(8,128)S(1)}, u32[]{:S(2)}, u32[]{:S(2)}) collective-permute-start(f32[30,512]{1,0:T(8,128)S(1)} %slice.263), channel_id=1, source_target_pairs={{4,0},{8,4},{12,8},{16,12},{20,16},{24,20},{28,24},{5,1},{9,5},{13... | collective-permute-start | bytes 184328 | tf_op jit(solution)/shard_map/ppermute | solution.py:10
  (2 other events, 1.8 us)
Sparse Core Ops, SparseCore 0:
  40.4 20.8 all-gather.5
  63.5 21.8 all-gather.3
  101.0 30.3 reduce-scatter.2
Sparse Core Ops, SparseCore 1:
  103.5 58.3 all-gather.7
  175.8 67.5 reduce-scatter.4
where the time goes:
time: 253 us; the launch traced here: 252 us
  waiting for transfers between devices  115 us (45%)
  blocking collectives  54.5 us (22%)
  matrix products  34.5 us (14%)
  local copies, waits for them, and re-layouts  18.2 us (7%)
  between operations  15.6 us (6%)
  other arithmetic  7.48 us (3%)
  starting transfers between devices  7.19 us (3%)
    reduce_scatter x1, waiting for transfers between devices, on_device(): lax.psum_scatter(lax.dot_general(columns, activated, (((0,), (0,)), ((),...  41.1 us
    reduce_scatter x1, waiting for transfers between devices, on_device(): lax.psum_scatter(partial_rows.astype(jnp.bfloat16).astype(jnp.float32).as...  30 us
    all_to_all x1, waiting for transfers between devices, on_device(): lax.all_to_all(shared, 'sp', split_axis=0, concat_axis=0, tiled=True)  21.8 us
    all_to_all x1, blocking collectives, on_device(): lax.all_to_all(send_rows, 'sp', split_axis=0, concat_axis=0, tiled=True)  21.6 us
    all_gather x1, waiting for transfers between devices, on_device(): lax.all_gather(part_routed, 'tp', axis=1, tiled=True)  19.1 us
    all_to_all x1, blocking collectives, on_device(): lax.all_to_all(send_routed, 'sp', split_axis=0, concat_axis=0, tiled=True)  17.5 us
    all_gather x1, blocking collectives, on_device(): mix_grad = lax.all_gather(grad_stream, 'tp', axis=1, tiled=True)  8.42 us
    psum x1, blocking collectives, on_device(): lax.psum((jnp.sum(normed_grad, axis=1), jnp.sum(normed_grad * normed, axi...  6.95 us
  transfers between devices with their start and end apart: 7, of which 5 were waited for; matrix products, arithmetic and copies ran while one was open for 11% of the time, Pallas kernels for 0%

commit v1 on v0

--- a/solution.py
+++ b/solution.py
@@ -56,6 +56,22 @@
     taps,
     w_proj,
 ):
+
+    def bench_make(x0, axis_name):
+        carry_out, d_next = (jax.lax.psum(1, axis_name), jax.lax.axis_index(axis_name))
+        block_now = x0.shape[0] // carry_out
+        state_next = jnp.roll(x0, -d_next * block_now, axis=0)
+        buffers = [lax.slice_in_dim(state_next, 0, block_now, axis=0)]
+        for rr in range(1, carry_out):
+            q_next = lax.slice_in_dim(state_next, rr * block_now, (rr + 1) * block_now, axis=0)
+            buffers.append(
+                jax.lax.ppermute(
+                    q_next, axis_name, [(c, (c + rr) % carry_out) for c in range(carry_out)]
+                )
+            )
+        plain = jnp.concatenate(buffers[::-1], axis=0)
+        return jnp.roll(plain, (d_next + 1) * buffers[0].shape[0], axis=0)
+
     devices = lax.axis_size("sp")
     local_tokens = routes.shape[0]
     top_count = routes.shape[1]
@@ -80,7 +96,7 @@
     send_rows, send_routed = (send_rows, send_routed)
     part_rows, part_routed = (
         lax.all_to_all(send_rows, "sp", split_axis=0, concat_axis=0, tiled=True),
-        lax.all_to_all(send_routed, "sp", split_axis=0, concat_axis=0, tiled=True),
+        bench_make(send_routed, "sp"),
     )
     expert_rows, routed_rows = (
         lax.all_gather(part_rows, "tp", axis=1, tiled=True),

time: 253 us -> 248 us (0.980)
  blocking collectives: 54.5 us -> 37 us
  starting transfers between devices: 7.19 us -> 16.2 us
  other arithmetic: 7.48 us -> 10.1 us
    all_to_all x1 -> x0, blocking collectives: 17.5 us -> none  [on_device(): lax.all_to_all(send_routed, 'sp', split_axis=0, concat_axis=0, tiled=True)]
    ppermute x0 -> x7, starting transfers between devices: none -> 9 us  [bench_make(): jax.lax.ppermute(q_next, axis_name, [(c, (c + rr) % carry_out) for c in r...]
    ppermute x0 -> x7, waiting for transfers between devices: none -> 7.14 us  [bench_make(): jax.lax.ppermute(q_next, axis_name, [(c, (c + rr) % carry_out) for c in r...]
  transfers between devices with their start and end apart: 7 -> 14, of which waited for: 5 -> 6; matrix products, arithmetic and copies ran while one was open for 11% -> 14% of each run, Pallas kernels for 0% -> 0%
where the time goes in v1:
time: 248 us
  waiting for transfers between devices  117 us (47%)
  blocking collectives  37 us (15%)
  matrix products  34.5 us (14%)
  local copies, waits for them, and re-layouts  17.2 us (7%)
  starting transfers between devices  16.2 us (7%)
  between operations  15.7 us (6%)
  other arithmetic  10.1 us (4%)
    reduce_scatter x1, waiting for transfers between devices, on_device(): lax.psum_scatter(lax.dot_general(columns, activated, (((0,), (0,)), ((),...  41 us
    reduce_scatter x1, waiting for transfers between devices, on_device(): lax.psum_scatter(partial_rows.astype(jnp.bfloat16).astype(jnp.float32).as...  30 us
    all_to_all x1, waiting for transfers between devices, on_device(): lax.all_to_all(shared, 'sp', split_axis=0, concat_axis=0, tiled=True)  21.8 us
    all_to_all x1, blocking collectives, on_device(): lax.all_to_all(send_rows, 'sp', split_axis=0, concat_axis=0, tiled=True)  21.6 us
    all_gather x1, waiting for transfers between devices, on_device(): lax.all_gather(part_routed, 'tp', axis=1, tiled=True)  16.7 us
    ppermute x7, starting transfers between devices, bench_make(): jax.lax.ppermute(q_next, axis_name, [(c, (c + rr) % carry_out) for c in r...  9 us
    all_gather x1, blocking collectives, on_device(): mix_grad = lax.all_gather(grad_stream, 'tp', axis=1, tiled=True)  8.42 us
    ppermute x7, waiting for transfers between devices, bench_make(): jax.lax.ppermute(q_next, axis_name, [(c, (c + rr) % carry_out) for c in r...  7.14 us
  transfers between devices with their start and end apart: 14, of which 6 were waited for; matrix products, arithmetic and copies ran while one was open for 14% of the time, Pallas kernels for 0%

profile of v1, /device:TPU:0, one launch (start us, length us, event | category | flops | bytes accessed | tf_op | source)
XLA Modules:
  0.0 247.8 jit_solution(7587946689600463595)
XLA Ops:
  10.9 2.1 gather_fusion.1
  13.4 21.6 %all_to_all.21 = bf16[8,60,512]{2,1,0:T(8,128)(2,1)S(1)} all-to-all(bf16[8,60,512]{2,1,0:T(8,128)(2,1)S(1)} %select_select_fusion), channel_id=1, replica_groups=mesh['sp'=8,'tp'=4] {'sp'}, dimensions={0} | all-to-all | bytes 983040 | tf_op jit(solution)/shard_map/all_to_all | solution.py:98
  37.2 2.1 gather_fusion
  40.5 2.4 collective-permute-start
  49.5 5.0 %collective-permute-done.3 = bf16[60,512]{1,0:T(8,128)(2,1)S(1)} collective-permute-done((bf16[60,512]{1,0:T(8,128)(2,1)S(1)}, bf16[60,512]{1,0:T(8,128)(2,1)S(1)}, u32[]{:S(2)}, u32[]{:S(2)}) %collective-permute-start.3) | collective-permute-done | bytes 61472 | tf_op jit(solution)/shard_map/ppermute | solution.py:68
  54.5 2.1 collective-permute-done.4
  59.4 4.9 %fusion.6 = f32[480,896]{1,0:T(8,128)S(1)} fusion(bf16[480,2048]{1,0:T(8,128)(2,1)} %all-gather.6.cloned.1.call-done, bf16[1,896,2048]{2,1,0:T(8,128)(2,1)} %param.20), kind=kOutput, calls=%fused_computation.39 | convolution fusion | flops 1761607680 | bytes 7356416 | tf_op jit(solution)/shard_map/dot_general | solution.py:18
  64.3 16.7 %all-gather.4.cloned.1.call-done = bf16[480,2048]{1,0:T(8,128)(2,1)} async-done(((bf16[480,512]{1,0:T(8,128)(2,1)}), bf16[480,2048]{1,0:T(8,128)(2,1)}) %all-gather.4.cloned.1.call-update) | async-done | bytes 1966096 | tf_op jit(solution)/shard_map/all_gather | solution.py:103
  81.0 5.1 %multiply_convert_fusion.2 = (bf16[480,896]{1,0:T(8,128)(2,1)S(1)}, f32[480,896]{1,0:T(8,128)S(1)}) fusion(f32[480,896]{1,0:T(8,128)S(1)} %fusion.6, bf16[480,2048]{1,0:T(8,128)(2,1)} %all-gather.4.cloned.1.call-done, bf16[1,896,2048]{2,1,0:T(8,128)(2,1)} %param.22), kind=kOutput, calls=%fused_computation.48 | convolution fusion | flops 1764188160 | bytes 9936896 | tf_op jit(solution)/shard_map/dot_general | solution.py:27
  87.0 2.2 fusion
  89.2 2.3 fusion.2
  92.7 3.7 %add_convert_fusion = bf16[480,2048]{1,0:T(8,128)(2,1)} fusion(f32[480,2048]{1,0:T(8,128)S(1)} %fusion, bf16[1,896,2048]{2,1,0:T(8,128)(2,1)S(1)} %copy-done.10, f32[480,896]{1,0:T(8,128)S(1)} %fusion.6, f32[480,896]{1,0:T(8,128)S(1)} %get-tuple-element.52, f32[480,896]{1,0:T(8,128)S(1)} %fusion.2), kind=kOutput, calls=%fused_computation.32 | convolution fusion | flops 1767874560 | bytes 14729216 | tf_op jit(solution)/shard_map/dot_general | solution.py:38
  97.1 30.0 %reduce-scatter.3.cloned.1.call-done = bf16[480,512]{1,0:T(8,128)(2,1)} async-done(((bf16[480,2048]{1,0:T(8,128)(2,1)}), bf16[480,512]{1,0:T(8,128)(2,1)}) %reduce-scatter.3.cloned.1.call-update) | async-done | bytes 491536 | tf_op jit(solution)/shard_map/reduce_scatter | solution.py:108
  128.9 5.5 %all-to-all-start.1 = ((bf16[8,60,512]{2,1,0:T(8,128)(2,1)}), bf16[8,60,512]{2,1,0:T(8,128)(2,1)S(1)}, u32[]{:S(2)}, u32[]{:S(2)}) async-start(bf16[8,60,512]{2,1,0:T(8,128)(2,1)} %all_to_all.16), calls=%async_computation.2 | async-start | bytes 1048576 | tf_op jit(solution)/shard_map/all_to_all | solution.py:114
  135.2 21.8 %all-to-all-done.1 = bf16[8,60,512]{2,1,0:T(8,128)(2,1)S(1)} async-done(((bf16[8,60,512]{2,1,0:T(8,128)(2,1)}), bf16[8,60,512]{2,1,0:T(8,128)(2,1)S(1)}, u32[]{:S(2)}, u32[]{:S(2)}) %all-to-all-start.1) | async-done | bytes 491552 | tf_op jit(solution)/shard_map/all_to_all | solution.py:114
  157.1 2.1 gather_fusion.2
  160.6 8.4 %all_gather.14 = bf16[192,2048]{1,0:T(8,128)(2,1)S(1)} all-gather(bf16[192,512]{1,0:T(8,128)(2,1)S(1)} %add_convert_fusion.1), channel_id=1, replica_groups=mesh['sp'=8,'tp'=4] {'tp'}, dimensions={1}, use_global_device_ids=true | all-gather | bytes 983040 | tf_op jit(solution)/shard_map/all_gather | solution.py:120
  169.0 2.3 convolution_convert_fusion
  172.9 6.0 %convert_bitcast_fusion = bf16[1,896,2048]{2,1,0:T(8,128)(2,1)} fusion(bf16[480,2048]{1,0:T(8,128)(2,1)S(1)} %copy-done.12, f32[480,896]{1,0:T(8,128)} %copy-done.17, f32[480,896]{1,0:T(8,128)} %copy-done.16), kind=kOutput, calls=%fused_computation.43 | convolution fusion | flops 1766023168 | bytes 9076736 | tf_op jit(solution)/shard_map/dot_general | solution.py:30
  178.9 2.5 fusion.123
  181.4 7.0 %all-reduce = (f32[192]{0:T(256)S(1)}, f32[192]{0:T(256)S(1)}) all-reduce(f32[192]{0:T(256)S(1)} %get-tuple-element.7, f32[192]{0:T(256)S(1)} %get-tuple-element.6), channel_id=1, replica_groups=mesh['sp'=8,'tp'=4] {'tp'}, use_global_device_ids=true, to_apply=%region_11.13 | all-reduce | flops 384 | bytes 3072 | tf_op jit(solution)/shard_map/psum | solution.py:141
  189.8 5.5 %convert_bitcast_fusion.1 = bf16[1,896,2048]{2,1,0:T(8,128)(2,1)} fusion(bf16[480,896]{1,0:T(8,128)(2,1)S(1)} %copy-done.19, bf16[480,2048]{1,0:T(8,128)(2,1)} %all-gather.6.cloned.1.call-done), kind=kOutput, calls=%fused_computation.44 | convolution fusion | flops 1763442688 | bytes 6496256 | tf_op jit(solution)/shard_map/dot_general | solution.py:35
  195.4 2.5 %fusion.22 = bf16[192,512]{1,0:T(8,128)(2,1)} fusion(f32[192,512]{1,0:T(8,128)S(1)} %subtract_multiply_fusion, f32[30,512]{1,0:T(8,128)S(1)} %collective-permute-done.7, f32[512]{0:T(512)S(1)} %bitcast.85, f32[512]{0:T(512)S(1)} %bitcast.86, f32[512]{0:T(512)S(1)} %bitcast.88, f32[512]{0:T(512)S(1)} %bitcast.89, f32[512]{0:T(512)S(1)} %bitcast.90, ...), kind=kLoop, calls=%fused_computation.101 | loop fusion | flops 9043968 | bytes 714752 | tf_op jit(solution)/shard_map/convert_element_type | solution.py:154
  197.9 41.0 %reduce-scatter.5.cloned.1.call-done = bf16[256,512]{1,0:T(8,128)(2,1)} async-done(((bf16[2048,512]{1,0:T(8,128)(2,1)}), bf16[256,512]{1,0:T(8,128)(2,1)}) %reduce-scatter.5.cloned.1.call-update) | async-done | bytes 262160 | tf_op jit(solution)/shard_map/reduce_scatter | solution.py:132
  (116 shorter events, 27.4 us)
Async XLA Ops:
  8.0 51.4 %all-gather.6.cloned.1.call-start = ((), (), s32[]{:S(2)}) async-start(), calls=%async_computation.5 | async-start | bytes 2457600 | tf_op jit(solution)/shard_map/all_gather | solution.py:102
  13.1 22.9 %copy-start.1 = (bf16[192,512]{1,0:T(8,128)(2,1)S(1)}, bf16[192,512]{1,0:T(8,128)(2,1)}, u32[]{:S(2)}) copy-start(bf16[192,512]{1,0:T(8,128)(2,1)} %param.17) | copy-start | bytes 589828
  35.9 45.0 %all-gather.4.cloned.1.call-start = ((), (), s32[]{:S(2)}) async-start(), calls=%async_computation.4 | async-start | bytes 2457600 | tf_op jit(solution)/shard_map/all_gather | solution.py:103
  40.5 7.3 %collective-permute-start = (bf16[60,512]{1,0:T(8,128)(2,1)S(1)}, bf16[60,512]{1,0:T(8,128)(2,1)S(1)}, u32[]{:S(2)}, u32[]{:S(2)}) collective-permute-start(bf16[60,512]{1,0:T(8,128)(2,1)S(1)} %get-tuple-element.17), channel_id=1, source_target_pairs={{0,28},{4,0},{8,4},{12,8},{16,12},{20,16},{24,20},{28,24},{1,29},{... | collective-permute-start | bytes 184328 | tf_op jit(solution)/shard_map/ppermute | solution.py:68
  42.9 5.7 %collective-permute-start.1 = (bf16[60,512]{1,0:T(8,128)(2,1)S(1)}, bf16[60,512]{1,0:T(8,128)(2,1)S(1)}, u32[]{:S(2)}, u32[]{:S(2)}) collective-permute-start(bf16[60,512]{1,0:T(8,128)(2,1)S(1)} %get-tuple-element.16), channel_id=1, source_target_pairs={{0,24},{4,28},{8,0},{12,4},{16,8},{20,12},{24,16},{28,20},{1,25},{... | collective-permute-start | bytes 184328 | tf_op jit(solution)/shard_map/ppermute | solution.py:68
  42.9 6.6 %collective-permute-start.2 = (bf16[60,512]{1,0:T(8,128)(2,1)S(1)}, bf16[60,512]{1,0:T(8,128)(2,1)S(1)}, u32[]{:S(2)}, u32[]{:S(2)}) collective-permute-start(bf16[60,512]{1,0:T(8,128)(2,1)S(1)} %get-tuple-element.15), channel_id=1, source_target_pairs={{0,20},{4,24},{8,28},{12,0},{16,4},{20,8},{24,12},{28,16},{1,21},{... | collective-permute-start | bytes 184328 | tf_op jit(solution)/shard_map/ppermute | solution.py:68
  44.6 9.9 %collective-permute-start.3 = (bf16[60,512]{1,0:T(8,128)(2,1)S(1)}, bf16[60,512]{1,0:T(8,128)(2,1)S(1)}, u32[]{:S(2)}, u32[]{:S(2)}) collective-permute-start(bf16[60,512]{1,0:T(8,128)(2,1)S(1)} %get-tuple-element.14), channel_id=1, source_target_pairs={{0,16},{4,20},{8,24},{12,28},{16,0},{20,4},{24,8},{28,12},{1,17},{... | collective-permute-start | bytes 184328 | tf_op jit(solution)/shard_map/ppermute | solution.py:68
  46.1 10.5 %collective-permute-start.4 = (bf16[60,512]{1,0:T(8,128)(2,1)S(1)}, bf16[60,512]{1,0:T(8,128)(2,1)S(1)}, u32[]{:S(2)}, u32[]{:S(2)}) collective-permute-start(bf16[60,512]{1,0:T(8,128)(2,1)S(1)} %get-tuple-element.13), channel_id=1, source_target_pairs={{0,12},{4,16},{8,20},{12,24},{16,28},{20,0},{24,4},{28,8},{1,13},{... | collective-permute-start | bytes 184328 | tf_op jit(solution)/shard_map/ppermute | solution.py:68
  47.9 8.8 %collective-permute-start.5 = (bf16[60,512]{1,0:T(8,128)(2,1)S(1)}, bf16[60,512]{1,0:T(8,128)(2,1)S(1)}, u32[]{:S(2)}, u32[]{:S(2)}) collective-permute-start(bf16[60,512]{1,0:T(8,128)(2,1)S(1)} %get-tuple-element.12), channel_id=1, source_target_pairs={{0,8},{4,12},{8,16},{12,20},{16,24},{20,28},{24,0},{28,4},{1,9},{5... | collective-permute-start | bytes 184328 | tf_op jit(solution)/shard_map/ppermute | solution.py:68
  48.6 8.0 %collective-permute-start.6 = (bf16[60,512]{1,0:T(8,128)(2,1)S(1)}, bf16[60,512]{1,0:T(8,128)(2,1)S(1)}, u32[]{:S(2)}, u32[]{:S(2)}) collective-permute-start(bf16[60,512]{1,0:T(8,128)(2,1)S(1)} %get-tuple-element.11), channel_id=1, source_target_pairs={{0,4},{4,8},{8,12},{12,16},{16,20},{20,24},{24,28},{28,0},{1,5},{5... | collective-permute-start | bytes 184328 | tf_op jit(solution)/shard_map/ppermute | solution.py:68
  59.1 67.9 %reduce-scatter.3.cloned.1.call-start = ((), (), s32[]{:S(2)}) async-start(), calls=%async_computation.6 | async-start | bytes 2457600 | tf_op jit(solution)/shard_map/reduce_scatter | solution.py:108
  64.3 27.3 %copy-start.16 = (f32[480,896]{1,0:T(8,128)}, f32[480,896]{1,0:T(8,128)S(1)}, u32[]{:S(2)}) copy-start(f32[480,896]{1,0:T(8,128)S(1)} %fusion.6) | copy-start | bytes 5160964
  96.4 38.2 %copy-start.5 = (s32[192,2]{0,1:T(2,128)S(1)}, s32[192,2]{0,1:T(2,128)}, u32[]{:S(2)}) copy-start(s32[192,2]{0,1:T(2,128)} %param.18) | copy-start | bytes 4612
  96.5 82.4 %all-gather.8.cloned.1.call-start = ((), (), s32[]{:S(2)}) async-start(), calls=%async_computation.8 | async-start | bytes 2359296 | tf_op jit(solution)/shard_map/all_gather | solution.py:128
  128.9 28.1 %all-to-all-start.1 = ((bf16[8,60,512]{2,1,0:T(8,128)(2,1)}), bf16[8,60,512]{2,1,0:T(8,128)(2,1)S(1)}, u32[]{:S(2)}, u32[]{:S(2)}) async-start(bf16[8,60,512]{2,1,0:T(8,128)(2,1)} %all_to_all.16), calls=%async_computation.2 | async-start | bytes 1048576 | tf_op jit(solution)/shard_map/all_to_all | solution.py:114
  134.4 104.5 %reduce-scatter.5.cloned.1.call-start = ((), (), s32[]{:S(2)}) async-start(), calls=%async_computation.7 | async-start | bytes 2359296 | tf_op jit(solution)/shard_map/reduce_scatter | solution.py:132
  159.2 9.8 %copy-start.3 = (bf16[192,512]{1,0:T(8,128)(2,1)S(1)}, bf16[192,512]{1,0:T(8,128)(2,1)}, u32[]{:S(2)}) copy-start(bf16[192,512]{1,0:T(8,128)(2,1)} %param.23) | copy-start | bytes 589828
  159.2 9.8 %copy-start.7 = (f32[192]{0:T(256)S(1)}, f32[192]{0:T(256)}, u32[]{:S(2)}) copy-start(f32[192]{0:T(256)} %param.25) | copy-start | bytes 2308
  159.2 9.8 %copy-start.8 = (f32[192]{0:T(256)S(1)}, f32[192]{0:T(256)}, u32[]{:S(2)}) copy-start(f32[192]{0:T(256)} %param.24) | copy-start | bytes 2308
  159.2 9.8 %copy-start.13 = (f32[512]{0:T(512)S(1)}, f32[512]{0:T(512)}, u32[]{:S(2)}) copy-start(f32[512]{0:T(512)} %param.27) | copy-start | bytes 6148
  159.2 9.8 %copy-start.14 = (f32[512]{0:T(512)S(1)}, f32[512]{0:T(512)}, u32[]{:S(2)}) copy-start(f32[512]{0:T(512)} %param.26) | copy-start | bytes 6148
  160.6 10.7 %copy-start.2 = (bf16[192,512]{1,0:T(8,128)(2,1)}, bf16[192,512]{1,0:T(8,128)(2,1)S(1)}, u32[]{:S(2)}) copy-start(bf16[192,512]{1,0:T(8,128)(2,1)S(1)} %add_convert_fusion.1) | copy-start | bytes 589828
  178.9 10.9 %copy-start.19 = (bf16[480,896]{1,0:T(8,128)(2,1)S(1)}, bf16[480,896]{1,0:T(8,128)(2,1)}, u32[]{:S(2)}) copy-start(bf16[480,896]{1,0:T(8,128)(2,1)} %copy-done.18) | copy-start | bytes 2580484
  188.5 6.9 %collective-permute-start.7 = (f32[30,512]{1,0:T(8,128)S(1)}, f32[30,512]{1,0:T(8,128)S(1)}, u32[]{:S(2)}, u32[]{:S(2)}) collective-permute-start(f32[30,512]{1,0:T(8,128)S(1)} %slice.303), channel_id=1, source_target_pairs={{4,0},{8,4},{12,8},{16,12},{20,16},{24,20},{28,24},{5,1},{9,5},{13... | collective-permute-start | bytes 184328 | tf_op jit(solution)/shard_map/ppermute | solution.py:10
  (10 other events, 26.9 us)
Sparse Core Ops, SparseCore 0:
  36.1 20.8 all-gather.5
  59.3 21.6 all-gather.3
  96.6 30.3 reduce-scatter.2
Sparse Core Ops, SparseCore 1:
  99.1 58.3 all-gather.7
  171.4 67.5 reduce-scatter.4
